TPU v7x, 256 devices: a 8x8x2 block of a 8x8x16 slice. The times are simulated.
256 devices in a mesh: grp: 2 (over z), ra: 16 (over y, core), cb: 8 (over x).
Axes of the slice: x: 8, y: 8, z: 2, core: 2. Of those that a mesh axis runs over, the one named last changes fastest.
The devices are a block of a 8x8x16 slice.
Arguments:
- tokens_in: bfloat16 [1024, 2048], P('grp', 'ra'), parts along dimension 0, may hold values from -40 to 40
- first_gain: float32 [2048], P('ra'), may hold values from 0.1 to 1.9
- first_gate: float32 [2048, 5632], P('ra', 'cb'), may hold values from -0.125 to 0.125
- first_gate_scale: float32 [5632], P('cb'), may hold values from 0.1 to 1.9
- first_up: float32 [2048, 5632], P('ra', 'cb'), may hold values from -0.125 to 0.125
- first_up_scale: float32 [5632], P('cb'), may hold values from 0.1 to 1.9
- first_down: float32 [5632, 2048], P('cb', 'ra'), may hold values from -0.078125 to 0.078125
- first_down_scale: float32 [2048], P('ra'), may hold values from 0.1 to 1.9
- second_gain: float32 [2048], P('ra'), may hold values from 0.1 to 1.9
- second_gate: float32 [2048, 5632], P('ra', 'cb'), may hold values from -0.125 to 0.125
- second_gate_scale: float32 [5632], P('cb'), may hold values from 0.1 to 1.9
- second_up: float32 [2048, 5632], P('ra', 'cb'), may hold values from -0.125 to 0.125
- second_up_scale: float32 [5632], P('cb'), may hold values from 0.1 to 1.9
- second_down: float32 [5632, 2048], P('cb', 'ra'), may hold values from -0.078125 to 0.078125
- second_down_scale: float32 [2048], P('ra'), may hold values from 0.1 to 1.9
Outputs:
- tokens_out: bfloat16 [1024, 2048], P('grp', 'ra'), parts along dimension 0
There are 2 independent parts, one for each index of `grp`. A program takes and returns all parts, laid end to end along the dimension named above; an argument that names none is the same for every part. Nothing has to cross between parts.
All inputs are finite; a program needn't handle non-finite values.
Results may differ from a plain program's by a relative error of at most 0.04.
Values may be sent and summed in bfloat16 or wider, within the bound.
A program may use at most 64 MiB of HBM per device.

v0:
```python
import jax
import jax.numpy as jnp
from jax import lax
from jax.sharding import PartitionSpec as P

D = 2048


def sent_to_all(shard, axis):
    peers = lax.axis_size(axis)
    return lax.all_to_all(
        jnp.broadcast_to(shard[None], (peers, *shard.shape)), axis, 0, 0, tiled=True
    )


def of_everyone(shard, axis):
    return sent_to_all(shard, axis).astype(jnp.float32).sum(axis=0)


def sent_together(arrays, axis, dim, along):
    columns = [a.reshape(*a.shape[:along], -1) for a in arrays]
    both = jnp.concatenate(columns, axis=along)
    result, at, outs = (lax.psum_scatter(both, axis, scatter_dimension=dim, tiled=True), 0, [])
    for a, column in zip(arrays, columns):
        slab = result[..., at : at + column.shape[along]]
        outs.append(slab.reshape(*slab.shape[:along], *a.shape[along:]))
        at += column.shape[along]
    return tuple(outs)


def cross_blocks(partial_value):
    return of_everyone(partial_value.astype(jnp.bfloat16), "cb").astype(jnp.float32)


def width_layer(acts, gain, gate_w, gate_s, up_w, up_s, down_w, down_s):
    acts_f = acts.astype(jnp.float32)
    squares = jnp.sum(acts_f * acts_f, axis=1)
    normed = (acts_f * gain).astype(jnp.bfloat16)
    gate_part = jnp.dot(normed, gate_w.astype(jnp.bfloat16), preferred_element_type=jnp.float32)
    up_part = jnp.dot(normed, up_w.astype(jnp.bfloat16), preferred_element_type=jnp.float32)
    total, gate_share, up_share = tuple(
        (
            part.astype(jnp.float32)
            for part in sent_together(
                (
                    squares.astype(jnp.bfloat16),
                    gate_part.astype(jnp.bfloat16),
                    up_part.astype(jnp.bfloat16),
                ),
                "ra",
                0,
                1,
            )
        )
    )
    factor = lax.rsqrt(total / D + 1e-06)[:, None]
    hidden_share = (jax.nn.silu(gate_share * factor * gate_s) * (up_share * factor * up_s)).astype(
        jnp.bfloat16
    )
    hidden = lax.all_gather(hidden_share, "ra", axis=0, tiled=True)
    partial_value = jnp.dot(hidden, down_w.astype(jnp.bfloat16), preferred_element_type=jnp.float32)
    partial_value = partial_value.astype(jnp.bfloat16).astype(jnp.float32)
    down = cross_blocks(partial_value) * down_s
    return (0.5 * acts_f + 0.5 * down).astype(jnp.bfloat16)


def local(
    tokens_in,
    first_gain,
    first_gate,
    first_gate_scale,
    first_up,
    first_up_scale,
    first_down,
    first_down_scale,
    second_gain,
    second_gate,
    second_gate_scale,
    second_up,
    second_up_scale,
    second_down,
    second_down_scale,
):
    middle = width_layer(
        tokens_in,
        first_gain,
        first_gate,
        first_gate_scale,
        first_up,
        first_up_scale,
        first_down,
        first_down_scale,
    )
    return width_layer(
        middle,
        second_gain,
        second_gate,
        second_gate_scale,
        second_up,
        second_up_scale,
        second_down,
        second_down_scale,
    )


def solution(mesh):
    return jax.shard_map(
        local,
        mesh=mesh,
        in_specs=(
            P("grp", "ra"),
            P("ra"),
            P("ra", "cb"),
            P("cb"),
            P("ra", "cb"),
            P("cb"),
            P("cb", "ra"),
            P("ra"),
            P("ra"),
            P("ra", "cb"),
            P("cb"),
            P("ra", "cb"),
            P("cb"),
            P("cb", "ra"),
            P("ra"),
        ),
        out_specs=P("grp", "ra"),
        check_vma=False,
    )
```

profile of v0, /device:TPU:513, one launch (start us, length us, event | category | flops | bytes accessed | tf_op | source)
XLA Modules:
  0.0 272.5 jit_solution(10470597815069633330)
XLA Ops:
  6.5 0.0 copy-start.1
  6.5 0.0 reduce-scatter.7.cloned.1.call-start
  6.6 1.1 fusion
  7.7 1.4 convolution_convert_fusion.3
  9.1 0.0 copy-done.1
  9.1 1.3 convolution_convert_fusion.2
  10.4 3.0 %concatenate.6 = bf16[512,1409]{0,1:T(8,128)(2,1)S(1)} concatenate(bf16[512,1]{0,1:T(2,128)(2,1)S(1)} %convert_element_type.118, bf16[512,704]{0,1:T(8,128)(2,1)S(1)} %convolution_convert_fusion.3, bf16[512,704]{0,1:T(8,128)(2,1)S(1)} %convolution_convert_fusion.2), dimensions={1} | concatenate | bytes 2885632 | tf_op jit(solution)/shard_map/concatenate | solution.py:22
  13.4 1.6 copy.24
  15.0 0.0 copy-start.6
  15.0 0.0 copy-start.7
  15.0 0.0 copy-start.2
  15.0 0.1 reduce-scatter.7.cloned.1.call-update
  15.0 0.1 reduce-scatter.9.cloned.1.call-start
  15.1 77.1 %reduce-scatter.7.cloned.1.call-done = bf16[32,1409]{1,0:T(8,128)(2,1)} async-done(((bf16[512,1409]{1,0:T(8,128)(2,1)}), bf16[32,1409]{1,0:T(8,128)(2,1)}) %reduce-scatter.7.cloned.1.call-update) | async-done | bytes 90192 | tf_op jit(solution)/shard_map/reduce_scatter | solution.py:23
  92.2 0.7 add_rsqrt_fusion.1
  92.9 0.1 copy.30
  93.0 0.0 copy-done.6
  93.0 0.0 copy-done.7
  93.0 1.0 multiply_convert_fusion.1
  94.0 19.6 %all_gather.6 = bf16[512,704]{1,0:T(8,128)(2,1)S(1)} all-gather(bf16[32,704]{1,0:T(8,128)(2,1)S(1)} %multiply_convert_fusion.1), channel_id=1, replica_groups=mesh['grp'=2,'ra'=16,'cb'=8] {'ra'}, dimensions={0}, use_global_device_ids=true | all-gather | bytes 765952 | tf_op jit(solution)/shard_map/all_gather | solution.py:60
  113.6 0.0 copy-done.2
  113.6 0.4 convolution_convert_fusion.5
  114.0 0.1 broadcast_in_dim.4
  114.1 0.0 copy-start
  114.1 0.0 copy-start.11
  114.2 0.0 copy-start.3
  114.2 0.0 copy-start.10
  114.2 35.3 %all_to_all.10 = bf16[8,512,128]{2,1,0:T(8,128)(2,1)S(1)} all-to-all(bf16[8,512,128]{2,1,0:T(8,128)(2,1)S(1)} %broadcast_in_dim.4), channel_id=1, replica_groups=mesh['grp'=2,'ra'=16,'cb'=8] {'cb'}, dimensions={0} | all-to-all | bytes 2097152 | tf_op jit(solution)/shard_map/all_to_all | solution.py:11
  149.4 0.0 copy-start.4
  149.4 0.1 convert_reduce_fusion.1
  149.6 0.0 copy-done
  149.6 0.0 copy-done.11
  149.6 0.2 fusion.4
  149.8 0.0 copy-done.3
  149.8 0.0 copy-done.10
  149.8 0.4 convolution_convert_fusion.1
  150.1 0.3 copy-done.4
  150.4 0.4 convolution_convert_fusion
  150.8 3.0 %concatenate.7 = bf16[512,1409]{0,1:T(8,128)(2,1)S(1)} concatenate(bf16[512,1]{0,1:T(2,128)(2,1)S(1)} %convert_element_type.134, bf16[512,704]{0,1:T(8,128)(2,1)S(1)} %convolution_convert_fusion.1, bf16[512,704]{0,1:T(8,128)(2,1)S(1)} %convolution_convert_fusion), dimensions={1} | concatenate | bytes 2885632 | tf_op jit(solution)/shard_map/concatenate | solution.py:22
  153.8 1.6 copy.26
  155.4 0.0 copy-start.8
  155.4 0.0 copy-start.9
  155.4 0.0 copy-start.5
  155.4 0.1 reduce-scatter.9.cloned.1.call-update
  155.4 52.3 %reduce-scatter.9.cloned.1.call-done = bf16[32,1409]{1,0:T(8,128)(2,1)} async-done(((bf16[512,1409]{1,0:T(8,128)(2,1)}), bf16[32,1409]{1,0:T(8,128)(2,1)}) %reduce-scatter.9.cloned.1.call-update) | async-done | bytes 90192 | tf_op jit(solution)/shard_map/reduce_scatter | solution.py:23
  207.7 0.7 add_rsqrt_fusion
  208.5 0.1 copy.31
  208.5 0.0 copy-done.8
  208.5 0.0 copy-done.9
  208.5 1.0 multiply_convert_fusion
  209.6 19.6 %all_gather.7 = bf16[512,704]{1,0:T(8,128)(2,1)S(1)} all-gather(bf16[32,704]{1,0:T(8,128)(2,1)S(1)} %multiply_convert_fusion), channel_id=1, replica_groups=mesh['grp'=2,'ra'=16,'cb'=8] {'ra'}, dimensions={0}, use_global_device_ids=true | all-gather | bytes 765952 | tf_op jit(solution)/shard_map/all_gather | solution.py:60
  229.2 0.0 copy-done.5
  229.2 0.4 convolution_convert_fusion.4
  229.6 0.1 broadcast_in_dim.5
  229.7 0.0 copy-start.12
  229.7 35.0 %all_to_all.11 = bf16[8,512,128]{2,1,0:T(8,128)(2,1)S(1)} all-to-all(bf16[8,512,128]{2,1,0:T(8,128)(2,1)S(1)} %broadcast_in_dim.5), channel_id=1, replica_groups=mesh['grp'=2,'ra'=16,'cb'=8] {'cb'}, dimensions={0} | all-to-all | bytes 2097152 | tf_op jit(solution)/shard_map/all_to_all | solution.py:11
  264.8 0.1 convert_reduce_fusion
  264.9 0.0 copy-done.12
  264.9 0.7 fusion.7
  (2 shorter events, 0.0 us)
Async XLA Ops:
  6.5 2.5 copy-start.1
  6.5 85.6 %reduce-scatter.7.cloned.1.call-start = ((), (), s32[]{:S(2)}) async-start(), calls=%async_computation.4 | async-start | bytes 1671168 | tf_op jit(solution)/shard_map/reduce_scatter | solution.py:23
  15.0 78.0 %copy-start.6 = (f32[704]{0:T(1024)S(1)}, f32[704]{0:T(1024)}, u32[]{:S(2)}) copy-start(f32[704]{0:T(1024)} %param.20) | copy-start | bytes 8452
  15.0 78.0 %copy-start.7 = (f32[704]{0:T(1024)S(1)}, f32[704]{0:T(1024)}, u32[]{:S(2)}) copy-start(f32[704]{0:T(1024)} %param.18) | copy-start | bytes 8452
  15.0 98.6 %copy-start.2 = (f32[704,128]{1,0:T(8,128)S(1)}, f32[704,128]{1,0:T(8,128)}, u32[]{:S(2)}) copy-start(f32[704,128]{1,0:T(8,128)} %param.21) | copy-start | bytes 1081348
  15.0 192.7 %reduce-scatter.9.cloned.1.call-start = ((), (), s32[]{:S(2)}) async-start(), calls=%async_computation.5 | async-start | bytes 1671168 | tf_op jit(solution)/shard_map/reduce_scatter | solution.py:23
  114.1 35.5 %copy-start = (bf16[512,128]{1,0:T(8,128)(2,1)S(1)}, bf16[512,128]{1,0:T(8,128)(2,1)}, u32[]{:S(2)}) copy-start(bf16[512,128]{1,0:T(8,128)(2,1)} %param.15) | copy-start | bytes 393220
  114.1 35.5 %copy-start.11 = (f32[128]{0:T(128)S(1)}, f32[128]{0:T(128)}, u32[]{:S(2)}) copy-start(f32[128]{0:T(128)} %param.22) | copy-start | bytes 1540
  114.2 35.6 %copy-start.3 = (f32[128,704]{0,1:T(8,128)S(1)}, f32[128,704]{0,1:T(8,128)}, u32[]{:S(2)}) copy-start(f32[128,704]{0,1:T(8,128)} %param.24) | copy-start | bytes 1081348
  114.2 35.6 %copy-start.10 = (f32[128]{0:T(128)S(1)}, f32[128]{0:T(128)}, u32[]{:S(2)}) copy-start(f32[128]{0:T(128)} %param.23) | copy-start | bytes 1540
  149.4 1.0 copy-start.4
  155.4 53.2 %copy-start.8 = (f32[704]{0:T(1024)S(1)}, f32[704]{0:T(1024)}, u32[]{:S(2)}) copy-start(f32[704]{0:T(1024)} %param.27) | copy-start | bytes 8452
  155.4 53.2 %copy-start.9 = (f32[704]{0:T(1024)S(1)}, f32[704]{0:T(1024)}, u32[]{:S(2)}) copy-start(f32[704]{0:T(1024)} %param.25) | copy-start | bytes 8452
  155.4 73.8 %copy-start.5 = (f32[704,128]{1,0:T(8,128)S(1)}, f32[704,128]{1,0:T(8,128)}, u32[]{:S(2)}) copy-start(f32[704,128]{1,0:T(8,128)} %param.28) | copy-start | bytes 1081348
  229.7 35.2 %copy-start.12 = (f32[128]{0:T(128)S(1)}, f32[128]{0:T(128)}, u32[]{:S(2)}) copy-start(f32[128]{0:T(128)} %param.29) | copy-start | bytes 1540
Sparse Core Ops, SparseCore 0:
  15.2 76.9 reduce-scatter.6
  155.6 52.1 reduce-scatter.8
where the time goes:
time: 273 us; the launch traced here: 272 us
  waiting for transfers between devices  129 us (47%)
  blocking collectives  110 us (40%)
  between operations  13.6 us (5%)
  local copies, waits for them, and re-layouts  9.94 us (4%)
  other arithmetic  5.68 us (2%)
  matrix products  4.13 us (2%)
    reduce_scatter x2, waiting for transfers between devices, sent_together(): lax.psum_scatter(both, axis, scatter_dimension=dim, tiled=True)  129 us
    all_to_all x2, blocking collectives, sent_to_all(): lax.all_to_all(jnp.broadcast_to(shard[None], (peers, *shard.shape)), axis...  70.3 us
    all_gather x2, blocking collectives, width_layer(): hidden = lax.all_gather(hidden_share, 'ra', axis=0, tiled=True)  39.3 us
    concatenate x2, local copies, waits for them, and re-layouts, sent_together(): both = jnp.concatenate(columns, axis=along)  6 us
  transfers between devices with their start and end apart: 2, of which 2 were waited for; matrix products, arithmetic and copies ran while one was open for 0% of the time, Pallas kernels for 0%

commit v1 on v0

v1 whole, which is shorter than its diff:
```python
import functools

import jax
import jax.numpy as jnp
from jax import lax
from jax.experimental import pallas as pl
from jax.experimental.pallas import tpu as pltpu
from jax.sharding import PartitionSpec as P

MESH = pl.DeviceIdType.MESH
BF16 = jnp.bfloat16
F32 = jnp.float32
LANES = 128
CHUNKS = 2
Y_SCATTER, SQUARES, Y_GATHER, X_SCATTER, X_GATHER = range(5)


def kernel(
    n_y, n_x, chunks,
    x_hbm, gain1_hbm, gate1_hbm, gate1_s_hbm, up1_hbm, up1_s_hbm, down1_hbm, down1_s_hbm,
    gain2_hbm, gate2_hbm, gate2_s_hbm, up2_hbm, up2_s_hbm, down2_hbm, down2_s_hbm,
    out_hbm,
    acts, other, gate_f, up_f, down_f, scale_f, vecs, vecs_sib,
    w_gu, w_d, scale_gu,
    part, part_in, sq, sq_in, hid, down_part, down_in, out_buf,
    load_sem, sib_send, sib_recv, send_sem, recv_sem, out_sem,
):
    tokens, width = x_hbm.shape
    ff = gate_f.shape[2]
    half = tokens // 2
    rows = half // chunks
    y_rows, x_rows = rows // n_y, rows // n_x
    main = ff // LANES * LANES
    tail = ff - main

    ra, x_at = lax.axis_index("ra"), lax.axis_index("cb")
    core = lax.rem(ra, 2)
    y_at = ra // 2
    sibling = {"ra": ra + 1 - 2 * core}

    def y_peer(o):
        return {"ra": 2 * lax.rem(y_at + o, n_y) + core}

    def x_peer(o):
        return {"cb": lax.rem(x_at + o, n_x)}

    def x_cross(o):
        return {"ra": ra + 1 - 2 * core, "cb": lax.rem(x_at + o, n_x)}

    def by_distance(n):
        return sorted(range(1, n), key=lambda o: -min(o, n - o))

    mine = pl.ds(pl.multiple_of(half * core, half), half)
    theirs = pl.ds(pl.multiple_of(half * (1 - core), half), half)
    copies = [
        (x_hbm.at[theirs], other),
        (x_hbm.at[mine], acts.at[0, :, pl.ds(0, width)]),
        (gate1_hbm, gate_f.at[0]),
        (up1_hbm, up_f.at[0]),
        (gain1_hbm, vecs.at[0]),
        (gain2_hbm, vecs.at[1]),
        (down1_s_hbm, vecs.at[2]),
        (down2_s_hbm, vecs.at[3]),
        (gate1_s_hbm, scale_f.at[0]),
        (up1_s_hbm, scale_f.at[1]),
        (gate2_s_hbm, scale_f.at[2]),
        (up2_s_hbm, scale_f.at[3]),
        (down1_hbm, down_f.at[0]),
        (gate2_hbm, gate_f.at[1]),
        (up2_hbm, up_f.at[1]),
        (down2_hbm, down_f.at[1]),
    ]
    loads = [pltpu.make_async_copy(s, d, load_sem.at[i]) for i, (s, d) in enumerate(copies)]
    for load in loads:
        load.start()

    barrier = pltpu.get_barrier_semaphore()
    peers = [sibling]
    peers += [y_peer(o) for o in range(1, n_y)]
    peers += [x_peer(o) for o in range(1, n_x)]
    peers += [x_cross(o) for o in range(1, n_x)]
    for peer in peers:
        pl.semaphore_signal(barrier, inc=1, device_id=peer, device_id_type=MESH)

    def pack_gate_up(l):
        own = pl.ds(0, width)
        w_gu[l, own, 0:main] = gate_f[l, :, 0:main].astype(BF16)
        w_gu[l, own, main : 2 * main] = up_f[l, :, 0:main].astype(BF16)
        w_gu[l, own, 2 * main : 2 * ff] = jnp.concatenate(
            [gate_f[l, :, main:ff], up_f[l, :, main:ff]], axis=1
        ).astype(BF16)

    def pack_scales(l):
        scale_gu[l, :, 0:main] = scale_f[2 * l, :, 0:main]
        scale_gu[l, :, main : 2 * main] = scale_f[2 * l + 1, :, 0:main]
        scale_gu[l, :, 2 * main : 2 * ff] = jnp.concatenate(
            [scale_f[2 * l, :, main:ff], scale_f[2 * l + 1, :, main:ff]], axis=1
        )

    def pack_down(l):
        w_d[l, 0:ff, 0:width] = down_f[l].astype(BF16)
        w_d[l, ff : main + LANES, :] = jnp.zeros((main + LANES - ff, 2 * width), BF16)

    def to_sibling(i, src, dst):
        return pltpu.make_async_remote_copy(
            src_ref=src, dst_ref=dst, send_sem=sib_send.at[i], recv_sem=sib_recv.at[i],
            device_id=sibling, device_id_type=MESH,
        )

    def gate_up_swap(i, l):
        return to_sibling(i, w_gu.at[l, pl.ds(0, width)], w_gu.at[l, pl.ds(width, width)])

    def down_swap(i, l):
        return to_sibling(
            i, w_d.at[l, pl.ds(0, ff), pl.ds(0, width)], w_d.at[l, pl.ds(0, ff), pl.ds(width, width)]
        )

    swaps = [
        to_sibling(0, other, acts.at[0, :, pl.ds(width, width)]),
        to_sibling(1, vecs, vecs_sib),
        gate_up_swap(2, 0),
        down_swap(3, 0),
        gate_up_swap(4, 1),
        down_swap(5, 1),
    ]

    def send(l, phase, j, src, dst, peer):
        pltpu.make_async_remote_copy(
            src_ref=src, dst_ref=dst, send_sem=send_sem.at[l, phase, j],
            recv_sem=recv_sem.at[l, phase, j], device_id=peer, device_id_type=MESH,
        ).start()

    def await_recv(l, phase, j, ref):
        pltpu.make_async_remote_copy(
            src_ref=ref, dst_ref=ref, send_sem=send_sem.at[l, phase, j],
            recv_sem=recv_sem.at[l, phase, j], device_id=sibling, device_id_type=MESH,
        ).wait_recv()

    def await_send(l, phase, j, ref):
        pltpu.make_async_remote_copy(
            src_ref=ref, dst_ref=ref, send_sem=send_sem.at[l, phase, j],
            recv_sem=recv_sem.at[l, phase, j], device_id=sibling, device_id_type=MESH,
        ).wait_send()

    def pair(i):
        return jnp.concatenate([vecs[i], vecs_sib[i]], axis=1)

    def gate_up(l, j):
        at = pl.ds(j * rows, rows)
        a = acts[l, at, :]
        gram = lax.dot_general(a, a, (((1,), (1,)), ((), ())), preferred_element_type=F32)
        r = lax.broadcasted_iota(jnp.int32, (rows, rows), 0)
        c = lax.broadcasted_iota(jnp.int32, (rows, rows), 1)
        sq[l, j] = jnp.sum(jnp.where(r == c, gram, 0.0), axis=0, keepdims=True)
        for o in by_distance(n_y):
            send(l, SQUARES, j, sq.at[l, j], sq_in.at[l, j, o - 1], y_peer(o))
        normed = (a.astype(F32) * pair(l)).astype(BF16)
        for n in range(0, 2 * ff, 2 * LANES):
            cols = slice(n, min(n + 2 * LANES, 2 * ff))
            part[l, at, cols] = jnp.dot(
                normed, w_gu[l, :, cols], preferred_element_type=F32
            ).astype(BF16)
        for o in by_distance(n_y):
            to = lax.rem(y_at + o, n_y)
            src = part.at[l, pl.ds(pl.multiple_of(j * rows + to * y_rows, y_rows), y_rows)]
            send(l, Y_SCATTER, j, src, part_in.at[l, j, o - 1], y_peer(o))

    def hidden(l, j):
        await_recv(l, SQUARES, j, sq_in.at[l, j])
        total = sq[l, j]
        for o in range(1, n_y):
            total = total + sq_in[l, j, o - 1]
        r = lax.broadcasted_iota(jnp.int32, (y_rows, rows), 0)
        c = lax.broadcasted_iota(jnp.int32, (y_rows, rows), 1)
        column = jnp.sum(jnp.where(c == r + y_at * y_rows, total, 0.0), axis=1, keepdims=True)
        factor = lax.rsqrt(column / (2 * width * n_y) + 1e-06)
        await_recv(l, Y_SCATTER, j, part_in.at[l, j])
        own = pl.ds(pl.multiple_of(j * rows + y_at * y_rows, y_rows), y_rows)

        def summed(cols):
            value = part[l, own, cols].astype(F32)
            for o in range(1, n_y):
                value = value + part_in[l, j, o - 1, :, cols].astype(F32)
            return value * factor * scale_gu[l, :, cols]

        for n in range(0, main, LANES):
            gate = summed(slice(n, n + LANES))
            up = summed(slice(main + n, main + n + LANES))
            hid[l, own, n : n + LANES] = (gate / (1.0 + jnp.exp(-gate)) * up).astype(BF16)
        gate = summed(slice(2 * main, 2 * ff))
        up = pltpu.roll(gate, tail, 1)
        lane = lax.broadcasted_iota(jnp.int32, (y_rows, LANES), 1)
        last = jnp.where(lane < tail, gate / (1.0 + jnp.exp(-gate)) * up, 0.0)
        hid[l, own, main : main + LANES] = last.astype(BF16)
        for o in by_distance(n_y):
            send(l, Y_GATHER, j, hid.at[l, own], hid.at[l, own], y_peer(o))

    def down(l, j):
        at = pl.ds(j * rows, rows)
        await_recv(l, Y_GATHER, j, hid.at[l, pl.ds(0, rows - y_rows)])
        value = jnp.dot(hid[l, at, :], w_d[l], preferred_element_type=F32)
        down_part[l, at, :] = value.astype(BF16)
        for o in by_distance(n_x):
            to = lax.rem(x_at + o, n_x)
            src = down_part.at[l, pl.ds(pl.multiple_of(j * rows + to * x_rows, x_rows), x_rows)]
            send(l, X_SCATTER, j, src, down_in.at[l, j, o - 1], x_peer(o))

    def result(l, j):
        await_recv(l, X_SCATTER, j, down_in.at[l, j])
        own = pl.ds(pl.multiple_of(j * rows + x_at * x_rows, x_rows), x_rows)
        value = down_part[l, own, :].astype(F32)
        for o in range(1, n_x):
            value = value + down_in[l, j, o - 1].astype(F32)
        value = 0.5 * acts[l, own, :].astype(F32) + 0.5 * (value * pair(2 + l))
        value = value.astype(BF16)
        if l == 0:
            acts[1, own, :] = value
            for o in by_distance(n_x):
                send(l, X_GATHER, j, acts.at[1, own], acts.at[1, own], x_peer(o))
        else:
            place = pl.ds(
                pl.multiple_of(half * core + j * rows + x_at * x_rows, x_rows), x_rows
            )
            out_buf[0, place, :] = value[:, 0:width]
            down_part[0, own, width : 2 * width] = value[:, width : 2 * width]
            across = down_part.at[0, own, pl.ds(width, width)]
            for o in by_distance(n_x):
                send(l, X_GATHER, j, out_buf.at[0, place], out_buf.at[0, place], x_peer(o))
                send(l, X_GATHER, j, across, out_buf.at[0, place], x_cross(o))
            send(l, X_GATHER, j, across, out_buf.at[0, place], sibling)

    for i in range(12):
        loads[i].wait()
    pack_gate_up(0)
    pl.semaphore_wait(barrier, len(peers))
    for i in range(3):
        swaps[i].start()
    pack_scales(0)
    pack_scales(1)
    loads[12].wait()
    pack_down(0)
    swaps[3].start()
    for i in range(3):
        swaps[i].wait_recv()
    for j in range(chunks):
        gate_up(0, j)
    loads[13].wait()
    loads[14].wait()
    pack_gate_up(1)
    swaps[4].start()
    loads[15].wait()
    pack_down(1)
    swaps[5].start()
    for l in range(2):
        for j in range(chunks):
            if l == 1:
                await_recv(0, X_GATHER, j, acts.at[1, pl.ds(0, rows - x_rows)])
                if j == 0:
                    swaps[4].wait_recv()
                gate_up(1, j)
        for j in range(chunks):
            hidden(l, j)
        for j in range(chunks):
            if j == 0:
                swaps[3 + 2 * l].wait_recv()
            down(l, j)
        if l == 1:
            for j in range(chunks):
                await_send(0, X_SCATTER, j, down_in.at[0, j])
        for j in range(chunks):
            result(l, j)
    stores = []
    for j in range(chunks):
        await_recv(1, X_GATHER, j, out_buf.at[0, pl.ds(0, 2 * rows - x_rows)])
        for h in range(2):
            at = pl.ds(h * half + j * rows, rows)
            store = pltpu.make_async_copy(out_buf.at[0, at], out_hbm.at[at], out_sem.at[j, h])
            store.start()
            stores.append(store)
    for swap in swaps:
        swap.wait_send()
    for l in range(2):
        for j in range(chunks):
            await_send(l, Y_SCATTER, j, part_in.at[l, j])
            await_send(l, SQUARES, j, sq_in.at[l, j])
            await_send(l, Y_GATHER, j, hid.at[l, pl.ds(0, rows - y_rows)])
            if l == 1:
                await_send(1, X_SCATTER, j, down_in.at[1, j])
                await_send(1, X_GATHER, j, out_buf.at[0, pl.ds(0, 2 * rows - x_rows)])
            else:
                await_send(0, X_GATHER, j, acts.at[1, pl.ds(0, rows - x_rows)])
    for store in stores:
        store.wait()


def local(n_y, n_x, *args):
    x, gate, down = args[0], args[2], args[6]
    tokens, width = x.shape
    ff = gate.shape[1]
    padded = ff // LANES * LANES + LANES
    half = tokens // 2
    rows = half // CHUNKS
    y_rows, x_rows = rows // n_y, rows // n_x
    flat = [a.reshape(1, -1) if a.ndim == 1 else a for a in args]
    dma = pltpu.SemaphoreType.DMA
    return pl.pallas_call(
        functools.partial(kernel, n_y, n_x, CHUNKS),
        name="half_steps",
        out_shape=jax.ShapeDtypeStruct(x.shape, x.dtype),
        in_specs=[pl.BlockSpec(memory_space=pl.ANY)] * len(flat),
        out_specs=pl.BlockSpec(memory_space=pl.ANY),
        scratch_shapes=[
            pltpu.VMEM((2, half, 2 * width), BF16),
            pltpu.VMEM((half, width), BF16),
            pltpu.VMEM((2, width, ff), F32),
            pltpu.VMEM((2, width, ff), F32),
            pltpu.VMEM((2, ff, width), F32),
            pltpu.VMEM((4, 1, ff), F32),
            pltpu.VMEM((4, 1, width), F32),
            pltpu.VMEM((4, 1, width), F32),
            pltpu.VMEM((2, 2 * width, 2 * ff), BF16),
            pltpu.VMEM((2, padded, 2 * width), BF16),
            pltpu.VMEM((2, 1, 2 * ff), F32),
            pltpu.VMEM((2, half, 2 * ff), BF16),
            pltpu.VMEM((2, CHUNKS, n_y - 1, y_rows, 2 * ff), BF16),
            pltpu.VMEM((2, CHUNKS, 1, rows), F32),
            pltpu.VMEM((2, CHUNKS, n_y - 1, 1, rows), F32),
            pltpu.VMEM((2, half, padded), BF16),
            pltpu.VMEM((2, half, 2 * width), BF16),
            pltpu.VMEM((2, CHUNKS, n_x - 1, x_rows, 2 * width), BF16),
            pltpu.VMEM((1, tokens, width), BF16),
            dma((16,)),
            dma((6,)),
            dma((6,)),
            dma((2, 5, CHUNKS)),
            dma((2, 5, CHUNKS)),
            dma((CHUNKS, 2)),
        ],
        compiler_params=pltpu.CompilerParams(collective_id=0, has_side_effects=True),
    )(*flat)


def solution(mesh):
    n_y, n_x = mesh.shape["ra"] // 2, mesh.shape["cb"]
    layer = (P("ra"), P("ra", "cb"), P("cb"), P("ra", "cb"), P("cb"), P("cb", "ra"), P("ra"))
    return jax.shard_map(
        functools.partial(local, n_y, n_x),
        mesh=mesh,
        in_specs=(P("grp", "ra"), *layer, *layer),
        out_specs=P("grp", "ra"),
        check_vma=False,
    )
```

time: 273 us -> 103 us (0.38)
  waiting for transfers between devices: 129 us -> 0 us
  blocking collectives: 110 us -> 0 us
  Pallas kernels: 0 us -> 93.3 us
  between operations: 13.6 us -> 0.02 us
  other arithmetic: 5.68 us -> 0 us
  matrix products: 4.13 us -> 0 us
    reduce_scatter x2 -> x0, waiting for transfers between devices: 129 us -> none  [sent_together(): lax.psum_scatter(both, axis, scatter_dimension=dim, tiled=True)]
    pallas_call x0 -> x1, Pallas kernels: none -> 93.3 us  [local(): pl.pallas_call(functools.partial(kernel, n_y, n_x, CHUNKS), name='half_st...]
    all_to_all x2 -> x0, blocking collectives: 70.3 us -> none  [sent_to_all(): lax.all_to_all(jnp.broadcast_to(shard[None], (peers, *shard.shape)), axis...]
    all_gather x2 -> x0, blocking collectives: 39.3 us -> none  [width_layer(): hidden = lax.all_gather(hidden_share, 'ra', axis=0, tiled=True)]
    concatenate x2 -> x0, local copies, waits for them, and re-layouts: 6 us -> none  [sent_together(): both = jnp.concatenate(columns, axis=along)]
    dot_general x6 -> x0, matrix products: 4.13 us -> none  [the longest x2 1.77 us: width_layer(): jnp.dot(normed, gate_w.astype(jnp.bfloat16), preferred_element_type=jnp.f...]
    unnamed x30 -> x19, local copies, waits for them, and re-layouts: 3.66 us -> 7.3 us
  transfers between devices with their start and end apart: 2 -> 0, of which waited for: 2 -> 0; matrix products, arithmetic and copies ran while one was open for 0% -> 0% of each run, Pallas kernels for 0% -> 0%
where the time goes in v1:
time: 103 us
  Pallas kernels  93.3 us (91%)
  local copies, waits for them, and re-layouts  9.65 us (9%)
    pallas_call x1, Pallas kernels, local(): pl.pallas_call(functools.partial(kernel, n_y, n_x, CHUNKS), name='half_st...  93.3 us
    unnamed x19, local copies, waits for them, and re-layouts  7.3 us
    reshape x4, local copies, waits for them, and re-layouts, local(): flat = [a.reshape(1, -1) if a.ndim == 1 else a for a in args]  2.36 us

profile of v1, /device:TPU:513, one launch (start us, length us, event | category | flops | bytes accessed | tf_op | source)
XLA Modules:
  0.0 103.0 jit_solution(13547360843481057726)
XLA Ops:
  0.0 0.0 copy-start.3
  0.0 0.0 copy-start.4
  0.0 0.7 copy-done.3
  0.7 0.6 reshape.25.gate1_s_hbm
  1.3 0.0 copy-done.4
  1.3 0.0 copy-start.5
  1.3 0.6 reshape.26.up1_s_hbm
  1.9 0.1 copy-done.5
  2.0 0.0 copy-start.6
  2.0 0.6 reshape.29.gate2_s_hbm
  2.6 0.1 copy-done.6
  2.7 0.6 reshape.30.up2_s_hbm
  3.2 0.0 copy-start
  3.2 2.0 %copy.16.gate1_hbm = f32[128,704]{1,0:T(8,128)} copy(f32[128,704]{0,1:T(8,128)} %param.17) | data formatting | bytes 720896 | tf_op args[2]
  5.2 0.0 copy-done
  5.2 0.0 copy-start.1
  5.2 0.9 copy.17.up1_hbm
  6.1 0.1 copy-done.1
  6.2 0.0 copy-start.2
  6.2 0.9 copy.18.gate2_hbm
  7.1 0.1 copy-done.2
  7.2 0.9 copy.19.up2_hbm
  8.1 93.3 %half_steps.1 = bf16[512,128]{1,0:T(8,128)(2,1)} custom-call(bf16[512,128]{1,0:T(8,128)(2,1)} %x_hbm.1, f32[1,128]{1,0:T(1,128)} %bitcast.4, f32[128,704]{1,0:T(8,128)} %copy.16.gate1_hbm, f32[1,704]{1,0:T(1,128)} %reshape.25.gate1_s_hbm, f32[128,704]{1,0:T(8,128)} %copy.17.up1_hbm, f32[1,704]{1,0:T(1,128)} %reshape.26.up1_s_hbm, f32[704,128]{1,0:T(8,128)} %down1_hbm.1, ...), custom_call_target="tpu_custom_call" | custom-call | tf_op jit(solution)/shard_map/half_steps/pallas_call | solution.py:306
  101.4 1.6 %copy.21 = bf16[512,128]{1,0:T(8,128)(2,1)} copy(bf16[512,128]{1,0:T(8,128)(2,1)} %half_steps.1) | data formatting | bytes 262144
Async XLA Ops:
  0.0 0.7 copy-start.3
  0.0 1.3 %copy-start.4 = (f32[704]{0:T(1024)S(1)}, f32[704]{0:T(1024)}, u32[]{:S(2)}) copy-start(f32[704]{0:T(1024)} %param.20) | copy-start | bytes 8452
  1.3 0.7 copy-start.5
  2.0 0.7 copy-start.6
  3.2 2.0 %copy-start = (f32[128,704]{0,1:T(8,128)S(1)}, f32[128,704]{0,1:T(8,128)}, u32[]{:S(2)}) copy-start(f32[128,704]{0,1:T(8,128)} %param.19) | copy-start | bytes 1081348
  5.2 1.0 copy-start.1
  6.2 1.0 copy-start.2

commit v2 on v1

--- a/solution.py
+++ b/solution.py
@@ -20,13 +20,13 @@
     x_hbm, gain1_hbm, gate1_hbm, gate1_s_hbm, up1_hbm, up1_s_hbm, down1_hbm, down1_s_hbm,
     gain2_hbm, gate2_hbm, gate2_s_hbm, up2_hbm, up2_s_hbm, down2_hbm, down2_s_hbm,
     out_hbm,
-    acts, other, gate_f, up_f, down_f, scale_f, vecs, vecs_sib,
+    acts, other, gate_f, up_f, down_f, scale_0, scale_1, scale_2, scale_3, vecs, vecs_sib,
     w_gu, w_d, scale_gu,
     part, part_in, sq, sq_in, hid, down_part, down_in, out_buf,
     load_sem, sib_send, sib_recv, send_sem, recv_sem, out_sem,
 ):
     tokens, width = x_hbm.shape
-    ff = gate_f.shape[2]
+    ff = gate_f.shape[1]
     half = tokens // 2
     rows = half // chunks
     y_rows, x_rows = rows // n_y, rows // n_x
@@ -61,10 +61,10 @@
         (gain2_hbm, vecs.at[1]),
         (down1_s_hbm, vecs.at[2]),
         (down2_s_hbm, vecs.at[3]),
-        (gate1_s_hbm, scale_f.at[0]),
-        (up1_s_hbm, scale_f.at[1]),
-        (gate2_s_hbm, scale_f.at[2]),
-        (up2_s_hbm, scale_f.at[3]),
+        (gate1_s_hbm, scale_0),
+        (up1_s_hbm, scale_1),
+        (gate2_s_hbm, scale_2),
+        (up2_s_hbm, scale_3),
         (down1_hbm, down_f.at[0]),
         (gate2_hbm, gate_f.at[1]),
         (up2_hbm, up_f.at[1]),
@@ -84,18 +84,17 @@
 
     def pack_gate_up(l):
         own = pl.ds(0, width)
-        w_gu[l, own, 0:main] = gate_f[l, :, 0:main].astype(BF16)
-        w_gu[l, own, main : 2 * main] = up_f[l, :, 0:main].astype(BF16)
-        w_gu[l, own, 2 * main : 2 * ff] = jnp.concatenate(
-            [gate_f[l, :, main:ff], up_f[l, :, main:ff]], axis=1
-        ).astype(BF16)
+        w_gu[l, 0:main, own] = gate_f[l, 0:main].astype(BF16)
+        w_gu[l, main : 2 * main, own] = up_f[l, 0:main].astype(BF16)
+        w_gu[l, 2 * main : main + ff, own] = gate_f[l, main:ff].astype(BF16)
+        w_gu[l, main + ff : 2 * ff, own] = up_f[l, main:ff].astype(BF16)
 
     def pack_scales(l):
-        scale_gu[l, :, 0:main] = scale_f[2 * l, :, 0:main]
-        scale_gu[l, :, main : 2 * main] = scale_f[2 * l + 1, :, 0:main]
-        scale_gu[l, :, 2 * main : 2 * ff] = jnp.concatenate(
-            [scale_f[2 * l, :, main:ff], scale_f[2 * l + 1, :, main:ff]], axis=1
-        )
+        gate_s, up_s = ((scale_0, scale_1), (scale_2, scale_3))[l]
+        scale_gu[l, 0, 0:main] = gate_s[0:main]
+        scale_gu[l, 0, main : 2 * main] = up_s[0:main]
+        scale_gu[l, 0, 2 * main : main + ff] = gate_s[main:ff]
+        scale_gu[l, 0, main + ff : 2 * ff] = up_s[main:ff]
 
     def pack_down(l):
         w_d[l, 0:ff, 0:width] = down_f[l].astype(BF16)
@@ -108,7 +107,7 @@
         )
 
     def gate_up_swap(i, l):
-        return to_sibling(i, w_gu.at[l, pl.ds(0, width)], w_gu.at[l, pl.ds(width, width)])
+        return to_sibling(i, w_gu.at[l, :, pl.ds(0, width)], w_gu.at[l, :, pl.ds(width, width)])
 
     def down_swap(i, l):
         return to_sibling(
@@ -157,8 +156,8 @@
         normed = (a.astype(F32) * pair(l)).astype(BF16)
         for n in range(0, 2 * ff, 2 * LANES):
             cols = slice(n, min(n + 2 * LANES, 2 * ff))
-            part[l, at, cols] = jnp.dot(
-                normed, w_gu[l, :, cols], preferred_element_type=F32
+            part[l, at, cols] = lax.dot_general(
+                normed, w_gu[l, cols], (((1,), (1,)), ((), ())), preferred_element_type=F32
             ).astype(BF16)
         for o in by_distance(n_y):
             to = lax.rem(y_at + o, n_y)
@@ -301,7 +300,9 @@
     half = tokens // 2
     rows = half // CHUNKS
     y_rows, x_rows = rows // n_y, rows // n_x
-    flat = [a.reshape(1, -1) if a.ndim == 1 else a for a in args]
+    flat = [a.reshape(1, -1) if a.shape == (width,) else a for a in args]
+    for i in (2, 4, 9, 11):
+        flat[i] = args[i].T
     dma = pltpu.SemaphoreType.DMA
     return pl.pallas_call(
         functools.partial(kernel, n_y, n_x, CHUNKS),
@@ -312,13 +313,16 @@
         scratch_shapes=[
             pltpu.VMEM((2, half, 2 * width), BF16),
             pltpu.VMEM((half, width), BF16),
-            pltpu.VMEM((2, width, ff), F32),
-            pltpu.VMEM((2, width, ff), F32),
             pltpu.VMEM((2, ff, width), F32),
-            pltpu.VMEM((4, 1, ff), F32),
+            pltpu.VMEM((2, ff, width), F32),
+            pltpu.VMEM((2, ff, width), F32),
+            pltpu.VMEM((ff,), F32),
+            pltpu.VMEM((ff,), F32),
+            pltpu.VMEM((ff,), F32),
+            pltpu.VMEM((ff,), F32),
             pltpu.VMEM((4, 1, width), F32),
             pltpu.VMEM((4, 1, width), F32),
-            pltpu.VMEM((2, 2 * width, 2 * ff), BF16),
+            pltpu.VMEM((2, 2 * ff, 2 * width), BF16),
             pltpu.VMEM((2, padded, 2 * width), BF16),
             pltpu.VMEM((2, 1, 2 * ff), F32),
             pltpu.VMEM((2, half, 2 * ff), BF16),

time: 103 us -> 95.2 us (0.924)
  local copies, waits for them, and re-layouts: 9.65 us -> 1.57 us
    unnamed x19 -> x1, local copies, waits for them, and re-layouts: 7.3 us -> 1.57 us
    reshape x4 -> x0, local copies, waits for them, and re-layouts: 2.36 us -> none  [local(): flat = [a.reshape(1, -1) if a.ndim == 1 else a for a in args]]
where the time goes in v2:
time: 95.2 us; the launch traced here: 95 us
  Pallas kernels  93.5 us (98%)
  local copies, waits for them, and re-layouts  1.57 us (2%)
    pallas_call x1, Pallas kernels, local(): pl.pallas_call(functools.partial(kernel, n_y, n_x, CHUNKS), name='half_st...  93.5 us

profile of v2, /device:TPU:513, one launch (start us, length us, event | category | flops | bytes accessed | tf_op | source)
XLA Modules:
  0.0 95.0 jit_solution(4422578899210450912)
XLA Ops:
  0.0 93.5 %half_steps.1 = bf16[512,128]{1,0:T(8,128)(2,1)} custom-call(bf16[512,128]{1,0:T(8,128)(2,1)} %x_hbm.1, f32[1,128]{1,0:T(1,128)} %bitcast.12, f32[704,128]{1,0:T(8,128)} %bitcast.8, f32[704]{0:T(1024)} %gate1_s_hbm.1, f32[704,128]{1,0:T(8,128)} %bitcast.9, f32[704]{0:T(1024)} %up1_s_hbm.1, f32[704,128]{1,0:T(8,128)} %down1_hbm.1, f32[1,128]{1,0:T(1,128)} %bitcast.13, ...), custom_call_target="tpu_custom_call" | custom-call | tf_op jit(solution)/shard_map/half_steps/pallas_call | solution.py:307
  93.5 1.6 %copy.17 = bf16[512,128]{1,0:T(8,128)(2,1)} copy(bf16[512,128]{1,0:T(8,128)(2,1)} %half_steps.1) | data formatting | bytes 262144

commit v3 on v2

--- a/solution.py
+++ b/solution.py
@@ -12,7 +12,7 @@
 F32 = jnp.float32
 LANES = 128
 CHUNKS = 2
-Y_SCATTER, SQUARES, Y_GATHER, X_SCATTER, X_GATHER = range(5)
+SQUARES, FOR_THREE, FOR_FOUR, FOR_ONE, FOR_TWO, FROM_TWO, FROM_REST, X_SCATTER, X_GATHER = range(9)
 
 
 def kernel(
@@ -22,7 +22,7 @@
     out_hbm,
     acts, other, gate_f, up_f, down_f, scale_0, scale_1, scale_2, scale_3, vecs, vecs_sib,
     w_gu, w_d, scale_gu,
-    part, part_in, sq, sq_in, hid, down_part, down_in, out_buf,
+    part, in_three, in_four, in_one, in_two, out_two, sq, sq_in, hid, down_part, down_in, out_buf,
     load_sem, sib_send, sib_recv, send_sem, recv_sem, out_sem,
 ):
     tokens, width = x_hbm.shape
@@ -39,13 +39,20 @@
     sibling = {"ra": ra + 1 - 2 * core}
 
     def y_peer(o):
-        return {"ra": 2 * lax.rem(y_at + o, n_y) + core}
+        return {"ra": 2 * lax.rem(y_at + o + n_y, n_y) + core}
 
     def x_peer(o):
         return {"cb": lax.rem(x_at + o, n_x)}
 
     def x_cross(o):
         return {"ra": ra + 1 - 2 * core, "cb": lax.rem(x_at + o, n_x)}
+
+    def y_share(j, o):
+        return pl.ds(pl.multiple_of(j * rows + lax.rem(y_at + o + n_y, n_y) * y_rows, y_rows), y_rows)
+
+    part_halves = (pl.ds(0, main), pl.ds(main, 2 * ff - main))
+    hid_half = (main + LANES) // 2 // LANES * LANES
+    hid_halves = (pl.ds(0, hid_half), pl.ds(hid_half, main + LANES - hid_half))
 
     def by_distance(n):
         return sorted(range(1, n), key=lambda o: -min(o, n - o))
@@ -159,10 +166,25 @@
             part[l, at, cols] = lax.dot_general(
                 normed, w_gu[l, cols], (((1,), (1,)), ((), ())), preferred_element_type=F32
             ).astype(BF16)
-        for o in by_distance(n_y):
-            to = lax.rem(y_at + o, n_y)
-            src = part.at[l, pl.ds(pl.multiple_of(j * rows + to * y_rows, y_rows), y_rows)]
-            send(l, Y_SCATTER, j, src, part_in.at[l, j, o - 1], y_peer(o))
+        for s, sign in enumerate((1, -1)):
+            cols = part_halves[s]
+            send(l, FOR_FOUR, j, part.at[l, y_share(j, 4), cols], in_four.at[l, j, :, cols], y_peer(2 * sign))
+        for s, sign in enumerate((1, -1)):
+            send(l, FOR_THREE, j, part.at[l, y_share(j, 3 * sign)], in_three.at[l, j, s], y_peer(sign))
+        for s, sign in enumerate((1, -1)):
+            send(l, FOR_ONE, j, part.at[l, y_share(j, sign)], in_one.at[l, j, s], y_peer(sign))
+
+    def combine(l, j):
+        await_recv(l, FOR_THREE, j, in_three.at[l, j])
+        await_recv(l, FOR_FOUR, j, in_four.at[l, j])
+        for s, sign in enumerate((1, -1)):
+            at = y_share(j, 2 * sign)
+            for h, cols in enumerate(part_halves):
+                value = part[l, at, cols].astype(F32) + in_three[l, j, s, :, cols].astype(F32)
+                if h == s:
+                    value = value + in_four[l, j, :, cols].astype(F32)
+                out_two[l, j, s, :, cols] = value.astype(BF16)
+            send(l, FOR_TWO, j, out_two.at[l, j, s], in_two.at[l, j, s], y_peer(2 * sign))
 
     def hidden(l, j):
         await_recv(l, SQUARES, j, sq_in.at[l, j])
@@ -173,13 +195,15 @@
         c = lax.broadcasted_iota(jnp.int32, (y_rows, rows), 1)
         column = jnp.sum(jnp.where(c == r + y_at * y_rows, total, 0.0), axis=1, keepdims=True)
         factor = lax.rsqrt(column / (2 * width * n_y) + 1e-06)
-        await_recv(l, Y_SCATTER, j, part_in.at[l, j])
-        own = pl.ds(pl.multiple_of(j * rows + y_at * y_rows, y_rows), y_rows)
+        await_recv(l, FOR_ONE, j, in_one.at[l, j])
+        await_recv(l, FOR_TWO, j, in_two.at[l, j])
+        own = y_share(j, 0)
 
         def summed(cols):
             value = part[l, own, cols].astype(F32)
-            for o in range(1, n_y):
-                value = value + part_in[l, j, o - 1, :, cols].astype(F32)
+            for s in range(2):
+                value = value + in_one[l, j, s, :, cols].astype(F32)
+                value = value + in_two[l, j, s, :, cols].astype(F32)
             return value * factor * scale_gu[l, :, cols]
 
         for n in range(0, main, LANES):
@@ -191,12 +215,23 @@
         lane = lax.broadcasted_iota(jnp.int32, (y_rows, LANES), 1)
         last = jnp.where(lane < tail, gate / (1.0 + jnp.exp(-gate)) * up, 0.0)
         hid[l, own, main : main + LANES] = last.astype(BF16)
-        for o in by_distance(n_y):
-            send(l, Y_GATHER, j, hid.at[l, own], hid.at[l, own], y_peer(o))
+        for sign in (1, -1):
+            send(l, FROM_TWO, j, hid.at[l, own], hid.at[l, own], y_peer(2 * sign))
+        for sign in (1, -1):
+            send(l, FROM_REST, j, hid.at[l, own], hid.at[l, own], y_peer(sign))
+
+    def forward(l, j):
+        await_recv(l, FROM_TWO, j, hid.at[l, pl.ds(0, 2 * y_rows)])
+        for s, sign in enumerate((1, -1)):
+            half_share = hid.at[l, y_share(j, -2 * sign), hid_halves[s]]
+            send(l, FROM_REST, j, half_share, half_share, y_peer(2 * sign))
+        for sign in (1, -1):
+            share = hid.at[l, y_share(j, -2 * sign)]
+            send(l, FROM_REST, j, share, share, y_peer(sign))
 
     def down(l, j):
         at = pl.ds(j * rows, rows)
-        await_recv(l, Y_GATHER, j, hid.at[l, pl.ds(0, rows - y_rows)])
+        await_recv(l, FROM_REST, j, hid.at[l, pl.ds(0, 5 * y_rows)])
         value = jnp.dot(hid[l, at, :], w_d[l], preferred_element_type=F32)
         down_part[l, at, :] = value.astype(BF16)
         for o in by_distance(n_x):
@@ -258,7 +293,11 @@
                     swaps[4].wait_recv()
                 gate_up(1, j)
         for j in range(chunks):
+            combine(l, j)
+        for j in range(chunks):
             hidden(l, j)
+        for j in range(chunks):
+            forward(l, j)
         for j in range(chunks):
             if j == 0:
                 swaps[3 + 2 * l].wait_recv()
@@ -280,9 +319,13 @@
         swap.wait_send()
     for l in range(2):
         for j in range(chunks):
-            await_send(l, Y_SCATTER, j, part_in.at[l, j])
             await_send(l, SQUARES, j, sq_in.at[l, j])
-            await_send(l, Y_GATHER, j, hid.at[l, pl.ds(0, rows - y_rows)])
+            await_send(l, FOR_THREE, j, in_three.at[l, j])
+            await_send(l, FOR_FOUR, j, in_four.at[l, j])
+            await_send(l, FOR_ONE, j, in_one.at[l, j])
+            await_send(l, FOR_TWO, j, in_two.at[l, j])
+            await_send(l, FROM_TWO, j, hid.at[l, pl.ds(0, 2 * y_rows)])
+            await_send(l, FROM_REST, j, hid.at[l, pl.ds(0, 5 * y_rows)])
             if l == 1:
                 await_send(1, X_SCATTER, j, down_in.at[1, j])
                 await_send(1, X_GATHER, j, out_buf.at[0, pl.ds(0, 2 * rows - x_rows)])
@@ -326,7 +369,11 @@
             pltpu.VMEM((2, padded, 2 * width), BF16),
             pltpu.VMEM((2, 1, 2 * ff), F32),
             pltpu.VMEM((2, half, 2 * ff), BF16),
-            pltpu.VMEM((2, CHUNKS, n_y - 1, y_rows, 2 * ff), BF16),
+            pltpu.VMEM((2, CHUNKS, 2, y_rows, 2 * ff), BF16),
+            pltpu.VMEM((2, CHUNKS, y_rows, 2 * ff), BF16),
+            pltpu.VMEM((2, CHUNKS, 2, y_rows, 2 * ff), BF16),
+            pltpu.VMEM((2, CHUNKS, 2, y_rows, 2 * ff), BF16),
+            pltpu.VMEM((2, CHUNKS, 2, y_rows, 2 * ff), BF16),
             pltpu.VMEM((2, CHUNKS, 1, rows), F32),
             pltpu.VMEM((2, CHUNKS, n_y - 1, 1, rows), F32),
             pltpu.VMEM((2, half, padded), BF16),
@@ -336,8 +383,8 @@
             dma((16,)),
             dma((6,)),
             dma((6,)),
-            dma((2, 5, CHUNKS)),
-            dma((2, 5, CHUNKS)),
+            dma((2, 9, CHUNKS)),
+            dma((2, 9, CHUNKS)),
             dma((CHUNKS, 2)),
         ],
         compiler_params=pltpu.CompilerParams(collective_id=0, has_side_effects=True),

time: 95.2 us -> 87.1 us (0.915)
  Pallas kernels: 93.5 us -> 85.4 us
    pallas_call x1, Pallas kernels: 93.5 us -> 85.4 us  [local(): pl.pallas_call(functools.partial(kernel, n_y, n_x, CHUNKS), name='half_st...]
where the time goes in v3:
time: 87.1 us; the launch traced here: 87 us
  Pallas kernels  85.4 us (98%)
  local copies, waits for them, and re-layouts  1.57 us (2%)
    pallas_call x1, Pallas kernels, local(): pl.pallas_call(functools.partial(kernel, n_y, n_x, CHUNKS), name='half_st...  85.4 us

profile of v3, /device:TPU:513, one launch (start us, length us, event | category | flops | bytes accessed | tf_op | source)
XLA Modules:
  0.0 87.0 jit_solution(15037891616883377405)
XLA Ops:
  0.0 85.4 %half_steps.1 = bf16[512,128]{1,0:T(8,128)(2,1)} custom-call(bf16[512,128]{1,0:T(8,128)(2,1)} %x_hbm.1, f32[1,128]{1,0:T(1,128)} %bitcast.12, f32[704,128]{1,0:T(8,128)} %bitcast.8, f32[704]{0:T(1024)} %gate1_s_hbm.1, f32[704,128]{1,0:T(8,128)} %bitcast.9, f32[704]{0:T(1024)} %up1_s_hbm.1, f32[704,128]{1,0:T(8,128)} %down1_hbm.1, f32[1,128]{1,0:T(1,128)} %bitcast.13, ...), custom_call_target="tpu_custom_call" | custom-call | tf_op jit(solution)/shard_map/half_steps/pallas_call | solution.py:350
  85.4 1.6 %copy.17 = bf16[512,128]{1,0:T(8,128)(2,1)} copy(bf16[512,128]{1,0:T(8,128)(2,1)} %half_steps.1) | data formatting | bytes 262144
